TPU v7x, 512 devices: a whole 4x4x16 slice. The times are simulated.
512 devices in a mesh: fs: 64 (over z, y), tp: 8 (over x, core).
Axes of the slice: x: 4, y: 4, z: 16, core: 2. Of those that a mesh axis runs over, the one named last changes fastest.
Arguments:
- cotangent: bfloat16 [8192, 2048], P('fs')
- values_first: bfloat16 [8192, 2048], P('fs', 'tp'), may hold values from -6 to 6
- values_second: bfloat16 [8192, 2048], P('fs', 'tp'), may hold values from -6 to 6
- head_lambda: float32 [16], P('tp'), may hold values from 0.3 to 0.8
- out_gain: float32 [128], replicated, may hold values from 0.3 to 3
- weight: float32 [2048, 2048], P('fs', 'tp'), may hold values from -0.125 to 0.125
- left_stat: float32 [2048, 2048], P('fs', 'tp'), as said below
- right_stat: float32 [16, 128, 128], P('tp')
- left_root: bfloat16 [2048, 2048], P('fs'), as said below
- right_root: bfloat16 [16, 128, 128], P('tp')
Outputs:
- update_step: float32 [2048, 2048], P('fs', 'tp')
- new_weight: float32 [2048, 2048], P('fs', 'tp')
- new_copy: bfloat16 [2048, 2048], P(None, 'tp')
- new_left_stat: float32 [2048, 2048], P('fs', 'tp')
- new_right_stat: float32 [16, 128, 128], P('tp')
Inputs may be any that keep to these rules, and one draw needn't show every extreme that they name: `left_root`: each of the 2048 x 2048 matrix and the 16 matrices of size 128 equals its transpose; the same holds for right_root. `left_stat`: the matrix and each of the 16 matrices equals its transpose; the same holds for right_stat.
All inputs are finite; a program needn't handle non-finite values.
Results may differ from a plain program's by a relative error of at most 0.007.
Values may be sent and summed in bfloat16 or wider, within the bound.
A program may use at most 64 MiB of HBM per device.

v0:
```python
import functools

import jax
import jax.numpy as jnp
from jax import lax
from jax.sharding import Mesh
from jax.sharding import PartitionSpec as P

TP = ("tp_0", "tp_1")
FS = ("fs_0", "fs_1")
FS_TP = ("fs_0", "fs_1", "tp_0", "tp_1")


epsilon = 1e-06
decay_rate = 0.9
learn_rate = 0.01
output_scale = 0.2


def reduced_to_own(pieces, axes, sequence):
    inside = pieces.shape[1:]
    pieces = pieces.reshape(*(lax.axis_size(a) for a in axes), *inside)
    pieces = jnp.moveaxis(pieces, sequence, range(len(axes))).reshape(-1, *inside)
    for k in sequence:
        pieces = lax.psum_scatter(pieces, axes[k], scatter_dimension=0, tiled=True)
    return pieces[0]


def cut_along(value, dim, size):
    dims = value.shape
    pieces = value.reshape(*dims[:dim], size, dims[dim] // size, *dims[dim + 1 :])
    return jnp.moveaxis(pieces, dim, 0)


def summed_rows(value, axes, sequence, dim):
    size = lax.axis_size(axes)
    return reduced_to_own(cut_along(value, dim, size), axes, sequence)


def gather_axes(value, axes, dim):
    if not axes:
        return value
    nearer = lax.all_gather(value, axes[-1], axis=dim, tiled=True)
    return gather_axes(nearer, axes[:-1], dim)


def summed_on_arrival(value, axis, dim):
    pieces = cut_along(value, dim, lax.axis_size(axis))
    arrived = lax.all_to_all(pieces, axis, split_axis=0, concat_axis=0, tiled=True)
    return arrived.astype(jnp.float32).sum(axis=0)


def by_axis(value, axes):
    return functools.reduce(lax.psum, axes, value)


def normalized(values_first, values_second, head_lambda, out_gain):
    token_count = values_first.shape[0]
    head_count = head_lambda.shape[0]
    head_size = out_gain.shape[0]
    first = values_first.astype(jnp.float32).reshape(token_count, head_count, head_size)
    second = values_second.astype(jnp.float32).reshape(token_count, head_count, head_size)
    difference = first - head_lambda[None, :, None] * second
    inverse = lax.rsqrt(jnp.mean(difference * difference, axis=-1, keepdims=True) + epsilon)
    scaled = difference * inverse * out_gain * output_scale
    return scaled.reshape(token_count, head_count * head_size).astype(jnp.bfloat16)


def by_head(matrix, head_count):
    return matrix.reshape(matrix.shape[0], head_count, matrix.shape[1] // head_count)


def head_products(matrix, head_count):
    heads = by_head(matrix, head_count)
    return jnp.einsum("rhi,rhj->hij", heads, heads, preferred_element_type=jnp.float32)


def shards(
    cotangent,
    values_first,
    values_second,
    head_lambda,
    out_gain,
    weight,
    left_stat,
    right_stat,
    left_root,
    right_root,
):
    head_count = head_lambda.shape[0]
    own_rows = weight.shape[0]
    own_cols = weight.shape[1]
    width = left_root.shape[1]
    total_cols = own_cols * lax.axis_size(TP)
    head_out = normalized(values_first, values_second, head_lambda, out_gain)
    contract_rows = (((0,), (0,)), ((), ()))
    contract_cols = (((1,), (1,)), ((), ()))
    gradient = summed_rows(
        lax.dot_general(cotangent, head_out, contract_rows, preferred_element_type=jnp.float32),
        FS,
        (1, 0),
        0,
    )
    grad_half = gradient.astype(jnp.bfloat16)
    portion = gather_axes(grad_half, FS, 0)
    left_acc = jnp.dot(left_root, portion, preferred_element_type=jnp.float32)
    products = lax.dot_general(
        grad_half, portion, contract_cols, preferred_element_type=jnp.float32
    )
    stat_cols = products
    right_acc = head_products(portion, head_count)
    left_acc, stat_cols, right_acc = (left_acc, stat_cols, right_acc)
    left_summed = summed_on_arrival(stat_cols.astype(jnp.bfloat16), TP, 1)
    new_left_stat = decay_rate * left_stat + (1.0 - decay_rate) / total_cols * left_summed
    new_right_stat = decay_rate * right_stat + (1.0 - decay_rate) / width * right_acc
    left_half = left_acc.astype(jnp.bfloat16)
    precond = jnp.einsum(
        "rhi,hij->rhj",
        by_head(left_half, head_count),
        right_root,
        preferred_element_type=jnp.float32,
    )
    precond = precond.reshape(own_rows, own_cols)
    grad_square, update_square = (
        by_axis(jnp.sum(gradient * gradient), FS_TP),
        by_axis(jnp.sum(precond * precond), FS_TP),
    )
    factor = jnp.sqrt((grad_square + epsilon) / (update_square + epsilon))
    update_step = factor * precond
    new_weight = weight - learn_rate * update_step
    new_copy = gather_axes(new_weight.astype(jnp.bfloat16), FS, 0)
    return (update_step, new_weight, new_copy, new_left_stat, new_right_stat)


def solution(mesh):
    finer = Mesh(mesh.devices.reshape(16, 4, 4, 2), ("fs_0", "fs_1", "tp_0", "tp_1"))
    in_specs = (
        P(FS, None),
        P(FS, TP),
        P(FS, TP),
        P(TP),
        P(),
        P(FS, TP),
        P(FS, TP),
        P(TP, None, None),
        P(FS, None),
        P(TP, None, None),
    )
    out_specs = (P(FS, TP), P(FS, TP), P(None, TP), P(FS, TP), P(TP, None, None))
    return jax.shard_map(
        shards, mesh=finer, in_specs=in_specs, out_specs=out_specs, check_vma=False
    )
```

profile of v0, /device:TPU:2, one launch (start us, length us, event | category | flops | bytes accessed | tf_op | source)
XLA Modules:
  0.0 358.9 jit_solution(10964241915965902323)
XLA Ops:
  7.2 1.0 reshape.47
  8.2 0.9 reshape.48
  9.1 0.7 broadcast_bitcast_fusion
  9.8 0.9 multiply_reduce_fusion
  10.8 0.2 mul.109
  11.0 1.3 convolution_bitcast_fusion
  12.4 1.8 copy.40
  14.2 3.2 copy.41
  17.4 0.0 reduce-scatter.5.cloned.1.call-start
  17.5 41.9 %reduce-scatter.3.cloned.1.call-done = f32[16,32,256]{2,1,0:T(8,128)} async-done(((f32[64,32,256]{2,1,0:T(8,128)}), f32[16,32,256]{2,1,0:T(8,128)}) %reduce-scatter.3.cloned.1.call-update) | async-done | bytes 524304 | tf_op jit(solution)/shard_map/reduce_scatter | solution.py:25
  59.5 72.8 %reduce-scatter.5.cloned.1.call-done = f32[1,32,256]{2,1,0:T(8,128)} async-done(((f32[16,32,256]{2,1,0:T(8,128)}), f32[1,32,256]{2,1,0:T(8,128)}) %reduce-scatter.5.cloned.1.call-update) | async-done | bytes 32784 | tf_op jit(solution)/shard_map/reduce_scatter | solution.py:25
  132.2 1.4 multiply_reduce_fusion.2
  133.7 12.9 %all-gather = bf16[1,128,256]{2,1,0:T(8,128)(2,1)} all-gather(bf16[1,32,256]{2,1,0:T(8,128)(2,1)S(1)} %get-tuple-element.17), channel_id=2, replica_groups=mesh['fs_0'=16,'fs_1'=4,'tp_0'=4,'tp_1'=2] {'fs_1'}, dimensions={1}, use_global_device_ids=true | all-gather | bytes 81920 | tf_op jit(solution)/shard_map/all_gather | solution.py:43
  146.6 0.0 all-gather.5.cloned.1.call-start
  146.6 67.8 %all-gather.7.cloned.1.call-done = bf16[1,2048,256]{2,1,0:T(8,128)(2,1)} async-done(((bf16[1,128,256]{2,1,0:T(8,128)(2,1)}), bf16[1,2048,256]{2,1,0:T(8,128)(2,1)}) %all-gather.7.cloned.1.call-update) | async-done | bytes 1048592 | tf_op jit(solution)/shard_map/all_gather | solution.py:43
  214.5 1.6 fusion.1
  216.1 0.7 multiply_reduce_fusion.1
  216.8 30.5 %all-reduce = (f32[]{:T(128)}, f32[]{:T(128)}) all-reduce(f32[]{:T(128)} %get-tuple-element.16, f32[]{:T(128)} %get-tuple-element.18), channel_id=1, replica_groups=mesh['fs_0'=16,'fs_1'=4,'tp_0'=4,'tp_1'=2] {'fs_0'}, use_global_device_ids=true, to_apply=%region_4.0 | all-reduce | flops 2 | bytes 16 | tf_op jit(solution)/shard_map/psum | solution.py:54
  247.3 11.1 %all-reduce.2 = (f32[]{:T(128)}, f32[]{:T(128)}) all-reduce(f32[]{:T(128)} %get-tuple-element.5, f32[]{:T(128)} %get-tuple-element.6), channel_id=1, replica_groups=mesh['fs_0'=16,'fs_1'=4,'tp_0'=4,'tp_1'=2] {'fs_1'}, use_global_device_ids=true, to_apply=%region_5.0 | all-reduce | flops 2 | bytes 16 | tf_op jit(solution)/shard_map/psum | solution.py:54
  258.4 9.2 %all-reduce.1 = (f32[]{:T(128)}, f32[]{:T(128)}) all-reduce(f32[]{:T(128)} %get-tuple-element.9, f32[]{:T(128)} %get-tuple-element.10), channel_id=1, replica_groups=mesh['fs_0'=16,'fs_1'=4,'tp_0'=4,'tp_1'=2] {'tp_0'}, use_global_device_ids=true, to_apply=%region_6.0 | all-reduce | flops 2 | bytes 16 | tf_op jit(solution)/shard_map/psum | solution.py:54
  267.6 3.1 all-reduce.3
  272.1 0.6 fusion.18
  272.7 12.6 %all_gather.14 = bf16[128,256]{1,0:T(8,128)(2,1)} all-gather(bf16[32,256]{1,0:T(8,128)(2,1)S(1)} %get-tuple-element.13), channel_id=1, replica_groups=mesh['fs_0'=16,'fs_1'=4,'tp_0'=4,'tp_1'=2] {'fs_1'}, dimensions={0}, use_global_device_ids=true | all-gather | bytes 81920 | tf_op jit(solution)/shard_map/all_gather | solution.py:43
  285.3 1.6 convolution_convert_fusion
  286.9 0.7 copy.64
  287.6 5.7 %all-to-all-start = ((bf16[8,32,256]{2,1,0:T(8,128)(2,1)}), bf16[8,32,256]{2,1,0:T(8,128)(2,1)S(1)}, u32[]{:S(2)}, u32[]{:S(2)}) async-start(bf16[8,32,256]{2,1,0:T(8,128)(2,1)} %bitcast.55), calls=%async_computation.2 | async-start | bytes 262144 | tf_op jit(solution)/shard_map/all_to_all | solution.py:49
  293.3 0.6 copy.45
  293.9 1.1 fusion
  295.0 2.9 all-to-all-done
  298.0 0.6 multiply_add_fusion
  298.6 51.5 %all-gather.5.cloned.1.call-done = bf16[2048,256]{1,0:T(8,128)(2,1)} async-done(((bf16[128,256]{1,0:T(8,128)(2,1)}), bf16[2048,256]{1,0:T(8,128)(2,1)}) %all-gather.5.cloned.1.call-update) | async-done | bytes 1048592 | tf_op jit(solution)/shard_map/all_gather | solution.py:43
  350.1 2.3 copy.66
  (22 shorter events, 0.2 us)
Async XLA Ops:
  7.2 3.8 %copy-start = (bf16[128,2048]{1,0:T(8,128)(2,1)S(1)}, bf16[128,2048]{1,0:T(8,128)(2,1)}, u32[]{:S(2)}) copy-start(bf16[128,2048]{1,0:T(8,128)(2,1)} %param.10) | copy-start | bytes 1572868
  7.2 52.2 %reduce-scatter.3.cloned.1.call-start = ((), (), s32[]{:S(2)}) async-start(), calls=%async_computation.3 | async-start | bytes 2621440 | tf_op jit(solution)/shard_map/reduce_scatter | solution.py:25
  17.4 197.1 %copy-start.2 = (bf16[32,2048]{1,0:T(8,128)(2,1)S(1)}, bf16[32,2048]{1,0:T(8,128)(2,1)}, u32[]{:S(2)}) copy-start(bf16[32,2048]{1,0:T(8,128)(2,1)} %param.18) | copy-start | bytes 393220
  17.4 198.7 %copy-start.4 = (bf16[2,128,128]{2,1,0:T(8,128)(2,1)S(1)}, bf16[2,128,128]{2,1,0:T(8,128)(2,1)}, u32[]{:S(2)}) copy-start(bf16[2,128,128]{2,1,0:T(8,128)(2,1)} %param.19) | copy-start | bytes 196612
  17.4 254.7 %copy-start.6 = (f32[32,256]{1,0:T(8,128)S(1)}, f32[32,256]{1,0:T(8,128)}, u32[]{:S(2)}) copy-start(f32[32,256]{1,0:T(8,128)} %param.15) | copy-start | bytes 98308
  17.4 114.8 %reduce-scatter.5.cloned.1.call-start = ((), (), s32[]{:S(2)}) async-start(), calls=%async_computation.4 | async-start | bytes 557056 | tf_op jit(solution)/shard_map/reduce_scatter | solution.py:25
  59.4 155.1 %all-gather.7.cloned.1.call-start = ((), (), s32[]{:S(2)}) async-start(), calls=%async_computation.6 | async-start | bytes 1114112 | tf_op jit(solution)/shard_map/all_gather | solution.py:43
  146.6 203.5 %all-gather.5.cloned.1.call-start = ((), (), s32[]{:S(2)}) async-start(), calls=%async_computation.5 | async-start | bytes 1114112 | tf_op jit(solution)/shard_map/all_gather | solution.py:43
  214.5 78.8 %copy-start.1 = (bf16[1,2048,256]{2,1,0:T(8,128)(2,1)S(1)}, bf16[1,2048,256]{2,1,0:T(8,128)(2,1)}, u32[]{:S(2)}) copy-start(bf16[1,2048,256]{2,1,0:T(8,128)(2,1)} %all-gather.7.cloned.1.call-done) | copy-start | bytes 3145732
  216.8 77.1 %copy-start.3 = (f32[2,128,128]{2,1,0:T(8,128)S(1)}, f32[2,128,128]{2,1,0:T(8,128)}, u32[]{:S(2)}) copy-start(f32[2,128,128]{2,1,0:T(8,128)} %param.17) | copy-start | bytes 393220
  287.6 10.3 %all-to-all-start = ((bf16[8,32,256]{2,1,0:T(8,128)(2,1)}), bf16[8,32,256]{2,1,0:T(8,128)(2,1)S(1)}, u32[]{:S(2)}, u32[]{:S(2)}) async-start(bf16[8,32,256]{2,1,0:T(8,128)(2,1)} %bitcast.55), calls=%async_computation.2 | async-start | bytes 262144 | tf_op jit(solution)/shard_map/all_to_all | solution.py:49
  293.3 4.7 %copy-start.5 = (f32[32,256]{1,0:T(8,128)S(1)}, f32[32,256]{1,0:T(8,128)}, u32[]{:S(2)}) copy-start(f32[32,256]{1,0:T(8,128)} %param.16) | copy-start | bytes 98308
Sparse Core Ops, SparseCore 0:
  17.5 41.8 reduce-scatter.2
  62.2 69.9 reduce-scatter.4
  146.7 67.7 all-gather.6
  285.4 64.6 all-gather.4
where the time goes:
time: 360 us; the launch traced here: 359 us
  waiting for transfers between devices  237 us (66%)
  blocking collectives  79.3 us (22%)
  between operations  15.2 us (4%)
  local copies, waits for them, and re-layouts  11.4 us (3%)
  matrix products  6.4 us (2%)
  starting transfers between devices  5.83 us (2%)
  other arithmetic  3.68 us (1%)
    all_gather x2, waiting for transfers between devices, gather_axes(): nearer = lax.all_gather(value, axes[-1], axis=dim, tiled=True)  119 us
    reduce_scatter x2, waiting for transfers between devices, reduced_to_own(): pieces = lax.psum_scatter(pieces, axes[k], scatter_dimension=0, tiled=True)  115 us
    psum x4, blocking collectives, by_axis(): return functools.reduce(lax.psum, axes, value)  53.8 us
    all_gather x2, blocking collectives, gather_axes(): nearer = lax.all_gather(value, axes[-1], axis=dim, tiled=True)  25.5 us
  transfers between devices with their start and end apart: 5, of which 5 were waited for; matrix products, arithmetic and copies ran while one was open for 1% of the time, Pallas kernels for 0%

commit v1 on v0

v1 whole, which is shorter than its diff:
```python
import jax
import jax.numpy as jnp
from jax import lax
from jax.experimental import pallas as pl
from jax.experimental.pallas import tpu as pltpu
from jax.sharding import Mesh
from jax.sharding import PartitionSpec as P

TP = ("tp_0", "tp_1")
FS = ("fs_0", "fs_1")
NZ, NY, NX, NC = 16, 4, 4, 2
NTP = NX * NC
ROWS = 32
COLS = 256
HEAD = 128
WIDTH = 2048
REACH = 4
FAR = (8, 7, 9, 6, 10, 5, 11)
NEAR = (3, 13, 2, 14, 1, 15)
ORDER = FAR + (4, 12) + NEAR + (0,)

epsilon = 1e-06
decay_rate = 0.9
learn_rate = 0.01
output_scale = 0.2

BF = jnp.bfloat16
F32 = jnp.float32


def rows_of(z, y):
    return pl.ds(pl.multiple_of(z * (NY * ROWS) + y * ROWS, ROWS), ROWS)


def around(position, step, size):
    return lax.rem(position + (step % size), size)


def send(src, dst, send_sem, recv_sem, device):
    return pltpu.make_async_remote_copy(
        src_ref=src,
        dst_ref=dst,
        send_sem=send_sem,
        recv_sem=recv_sem,
        device_id=device,
        device_id_type=pl.DeviceIdType.MESH,
    )


class Spread:
    def __init__(self, buf, place, sems, at):
        self.buf, self.place = buf, place
        self.zs, self.zr, self.ys, self.yr = sems
        self.at = at
        self.open = []

    def block(self, step):
        z, y, x, c = self.at
        return self.buf.at[self.place(around(z, -step, NZ), y)]

    def hop(self, step, reach, down):
        z, y, x, c = self.at
        there = around(z, -reach if down else reach, NZ)
        arrives = (step - reach if down else step + reach) % NZ
        block = self.block(step)
        return send(block, block, self.zs.at[arrives], self.zr.at[arrives], (there, y, x, c))

    def launch(self, step, reaches, down):
        for reach in reaches:
            copy = self.hop(step, reach, down)
            copy.start()
            self.open.append(copy)

    def begin(self):
        for reach in (4, 3, 2, 1):
            self.launch(0, (reach,), False)
            self.launch(0, (reach,), True)

    def wait(self, step):
        block = self.block(step)
        z, y, x, c = self.at
        send(block, block, self.zs.at[step], self.zr.at[step], (around(z, 1, NZ), y, x, c)).wait_recv()

    def relay(self):
        self.launch(4, (4, 3, 2, 1), False)
        self.launch(12, (3, 2, 1), True)

    def across(self, step):
        z, y, x, c = self.at
        block = self.block(step)
        for far in (2, 1, 3):
            copy = send(block, block, self.ys.at[far, step], self.yr.at[far, step], (z, around(y, far, NY), x, c))
            copy.start()
            self.open.append(copy)

    def wait_across(self):
        z, y, x, c = self.at
        for step in range(NZ):
            for far in (1, 2, 3):
                block = self.buf.at[self.place(around(z, -step, NZ), around(y, -far, NY))]
                send(
                    block, block, self.ys.at[far, step], self.yr.at[far, step], (z, around(y, far, NY), x, c)
                ).wait_recv()

    def drain(self):
        for copy in self.open:
            copy.wait_send()


def kernel(
    cot,
    first,
    second,
    lam,
    gain,
    weight,
    left_stat,
    right_stat,
    left_root,
    right_root,
    update_step,
    new_weight,
    new_copy,
    new_left_stat,
    new_right_stat,
    head_out,
    partial,
    partial_half,
    from_y,
    to_z,
    from_z1,
    from_z2,
    held_weight,
    portion,
    held_step,
    stat_out,
    stat_in,
    scal_z,
    scal_y,
    scal_t,
    rys,
    ryr,
    rzs,
    rzr,
    r2s,
    r2r,
    wzs,
    wzr,
    wys,
    wyr,
    gzs,
    gzr,
    gys,
    gyr,
    pzs,
    pzr,
    pys,
    pyr,
    szs,
    szr,
    sys_,
    syr,
    sts,
    str_,
    lts,
    ltr,
):
    z, y, x, c = (lax.axis_index(a) for a in ("fs_0", "fs_1", "tp_0", "tp_1"))
    at = (z, y, x, c)
    me = x * NC + c

    def z_device(step):
        return (around(z, step, NZ), y, x, c)

    def y_device(step):
        return (z, around(y, step, NY), x, c)

    def t_index(step):
        return around(me, step, NTP)

    def t_device(step):
        other = t_index(step)
        return (z, y, other // NC, lax.rem(other, NC))

    barrier = pltpu.get_barrier_semaphore()
    peers = [z_device(s) for s in (1, 2, 3, 4, 12, 13, 14, 15)]
    peers += [y_device(s) for s in (1, 2, 3)]
    peers += [t_device(s) for s in range(1, NTP)]
    for peer in peers:
        pl.semaphore_signal(barrier, inc=1, device_id=peer, device_id_type=pl.DeviceIdType.MESH)

    held_weight[rows_of(z, y)] = weight[...].astype(BF)
    for h in range(COLS // HEAD):
        lanes = slice(h * HEAD, (h + 1) * HEAD)
        difference = first[:, lanes].astype(F32) - lam[h] * second[:, lanes].astype(F32)
        mean = jnp.mean(difference * difference, axis=-1, keepdims=True)
        scaled = difference * lax.rsqrt(mean + epsilon) * gain[...] * output_scale
        head_out[:, lanes] = scaled.astype(BF)

    pl.semaphore_wait(barrier, len(peers))

    def by_rows(zz, yy):
        return rows_of(zz, yy)

    weights = Spread(held_weight, by_rows, (wzs, wzr, wys, wyr), at)
    weights.begin()

    drain = []
    for step in ORDER:
        zz = around(z, step, NZ)
        tokens = cot[:, pl.ds(pl.multiple_of(zz * HEAD, HEAD), HEAD)]
        block = lax.dot_general(
            tokens, head_out[...], (((0,), (0,)), ((), ())), preferred_element_type=F32
        )
        rows = pl.ds(pl.multiple_of(zz * HEAD, HEAD), HEAD)
        partial[rows] = block
        partial_half[rows] = block.astype(BF)
        for far in (2, 1, 3):
            copy = send(
                partial_half.at[rows_of(zz, around(y, far, NY))],
                from_y.at[far, step],
                rys.at[far, step],
                ryr.at[far, step],
                y_device(far),
            )
            copy.start()
            drain.append(copy)

    def summed(step):
        zz = around(z, step, NZ)
        total = partial[rows_of(zz, y)]
        for far in (1, 3, 2):
            send(
                from_y.at[far, step], from_y.at[far, step], rys.at[far, step], ryr.at[far, step], y_device(far)
            ).wait_recv()
            total = total + from_y[far, step].astype(F32)
        return total

    for step in FAR:
        to_z[step] = summed(step).astype(BF)
        via = step - REACH if step <= NZ // 2 else step + REACH
        copy = send(to_z.at[step], from_z1.at[via], rzs.at[step], rzr.at[via], z_device(via))
        copy.start()
        drain.append(copy)
    for step in NEAR:
        to_z[step] = summed(step).astype(BF)
        copy = send(to_z.at[step], from_z2.at[step], r2s.at[step], r2r.at[step], z_device(step))
        copy.start()
        drain.append(copy)
    for step in (0, 1, 15, 2, 14, 3, 13):
        if step:
            weights.wait(step)
        weights.across(step)
    weights.wait(4)
    weights.wait(12)
    weights.relay()
    for step, vias in ((4, (4, 3, 2, 1)), (12, (13, 14, 15))):
        total = summed(step)
        for via in sorted(vias, key=lambda v: min(v, NZ - v)):
            send(to_z.at[via], from_z1.at[via], rzs.at[via], rzr.at[via], z_device(via)).wait_recv()
            total = total + from_z1[via].astype(F32)
        to_z[step] = total.astype(BF)
        copy = send(to_z.at[step], from_z2.at[step], r2s.at[step], r2r.at[step], z_device(step))
        copy.start()
        drain.append(copy)
    own = summed(0)
    weights.across(4)
    weights.across(12)
    for step in (5, 11, 6, 10, 7, 9, 8):
        weights.wait(step)
        weights.across(step)
    for step in (1, 15, 2, 14, 3, 13, 4, 12):
        send(to_z.at[step], from_z2.at[step], r2s.at[step], r2r.at[step], z_device(step)).wait_recv()
        own = own + from_z2[step].astype(F32)

    own_half = own.astype(BF)
    portion[rows_of(z, y)] = own_half
    grads = Spread(portion, by_rows, (gzs, gzr, gys, gyr), at)
    grads.begin()
    grads.across(0)
    grad_square = jnp.sum(own * own, axis=(0, 1), keepdims=True)
    for step in (1, 15, 2, 14, 3, 13):
        grads.wait(step)
        grads.across(step)
    grads.wait(4)
    grads.wait(12)
    grads.relay()
    grads.across(4)
    grads.across(12)
    for step in (5, 11, 6, 10, 7, 9, 8):
        grads.wait(step)
        grads.across(step)
    grads.wait_across()

    left_half = jnp.dot(left_root[...], portion[...], preferred_element_type=F32).astype(BF)
    steps = [
        jnp.dot(left_half[:, h * HEAD : (h + 1) * HEAD], right_root[h], preferred_element_type=F32)
        for h in range(COLS // HEAD)
    ]
    precond = jnp.concatenate(steps, axis=1)
    held_step[rows_of(z, y)] = precond.astype(BF)
    places = Spread(held_step, by_rows, (pzs, pzr, pys, pyr), at)
    places.begin()
    places.across(0)
    step_square = jnp.sum(precond * precond, axis=(0, 1), keepdims=True)
    top = lax.broadcasted_iota(jnp.int32, (8, HEAD), 0) < 4
    scal_z[z] = jnp.where(top, jnp.broadcast_to(step_square, (8, HEAD)), jnp.broadcast_to(grad_square, (8, HEAD)))
    scalars = Spread(scal_z, lambda zz, yy: zz, (szs, szr, None, None), at)
    scalars.begin()

    for j in range(NTP):
        stat_out[j] = lax.dot_general(
            own_half,
            portion[j * COLS : (j + 1) * COLS],
            (((1,), (1,)), ((), ())),
            preferred_element_type=F32,
        )
    for far in range(1, NTP):
        copy = send(
            stat_out.at[t_index(far)], stat_in.at[far], lts.at[far], ltr.at[far], t_device(far)
        )
        copy.start()
        drain.append(copy)
    for h in range(COLS // HEAD):
        lanes = slice(h * HEAD, (h + 1) * HEAD)
        product = lax.dot_general(
            portion[:, lanes], portion[:, lanes], (((0,), (0,)), ((), ())), preferred_element_type=F32
        )
        new_right_stat[h] = decay_rate * right_stat[h] + (1.0 - decay_rate) / WIDTH * product

    for step in (1, 15, 2, 14, 3, 13):
        places.wait(step)
        places.across(step)
    places.wait(4)
    places.wait(12)
    places.relay()
    scalars.wait(4)
    scalars.wait(12)
    scalars.relay()
    places.across(4)
    places.across(12)
    stat = stat_out[me]
    for far in range(1, NTP):
        send(
            stat_out.at[t_index(far)], stat_in.at[far], lts.at[far], ltr.at[far], t_device(far)
        ).wait_recv()
        stat = stat + stat_in[far]
    new_left_stat[...] = decay_rate * left_stat[...] + (1.0 - decay_rate) / WIDTH * stat
    for step in (5, 11, 6, 10, 7, 9, 8):
        places.wait(step)
        places.across(step)
    for step in (1, 15, 2, 14, 3, 13, 5, 11, 6, 10, 7, 9, 8):
        scalars.wait(step)
    total = scal_z[0]
    for k in range(1, NZ):
        total = total + scal_z[k]
    scal_y[y] = total
    for far in (2, 1, 3):
        copy = send(scal_y.at[y], scal_y.at[y], sys_.at[far], syr.at[far], y_device(far))
        copy.start()
        drain.append(copy)
    for far in (1, 3, 2):
        block = scal_y.at[around(y, -far, NY)]
        send(block, block, sys_.at[far], syr.at[far], y_device(far)).wait_recv()
    total = scal_y[0]
    for k in range(1, NY):
        total = total + scal_y[k]
    scal_t[me] = total
    for far in range(1, NTP):
        copy = send(scal_t.at[me], scal_t.at[me], sts.at[far], str_.at[far], t_device(far))
        copy.start()
        drain.append(copy)
    for far in range(1, NTP):
        block = scal_t.at[t_index(-far)]
        send(block, block, sts.at[far], str_.at[far], t_device(far)).wait_recv()
    total = scal_t[0]
    for k in range(1, NTP):
        total = total + scal_t[k]
    factor = jnp.sqrt((total[4:5, 0:1] + epsilon) / (total[0:1, 0:1] + epsilon))

    step_own = factor * precond
    update_step[...] = step_own
    new_weight[...] = weight[...] - learn_rate * step_own
    weights.wait_across()
    places.wait_across()
    scale = learn_rate * factor
    for k in range(NZ):
        rows = pl.ds(k * HEAD, HEAD)
        new_copy[rows] = (held_weight[rows].astype(F32) - scale * held_step[rows].astype(F32)).astype(BF)

    for copy in drain:
        copy.wait_send()
    for spread in (weights, grads, places, scalars):
        spread.drain()


def shards(
    cotangent,
    values_first,
    values_second,
    head_lambda,
    out_gain,
    weight,
    left_stat,
    right_stat,
    left_root,
    right_root,
):
    vmem = pl.BlockSpec(memory_space=pltpu.VMEM)
    smem = pl.BlockSpec(memory_space=pltpu.SMEM)
    dma = pltpu.SemaphoreType.DMA
    spread = [dma((NZ,)), dma((NZ,)), dma((NY, NZ)), dma((NY, NZ))]
    return pl.pallas_call(
        kernel,
        out_shape=(
            jax.ShapeDtypeStruct((ROWS, COLS), F32),
            jax.ShapeDtypeStruct((ROWS, COLS), F32),
            jax.ShapeDtypeStruct((WIDTH, COLS), BF),
            jax.ShapeDtypeStruct((ROWS, COLS), F32),
            jax.ShapeDtypeStruct((COLS // HEAD, HEAD, HEAD), F32),
        ),
        in_specs=[vmem, vmem, vmem, smem] + [vmem] * 6,
        out_specs=[vmem] * 5,
        scratch_shapes=[
            pltpu.VMEM((128, COLS), BF),
            pltpu.VMEM((WIDTH, COLS), F32),
            pltpu.VMEM((WIDTH, COLS), BF),
            pltpu.VMEM((NY, NZ, ROWS, COLS), BF),
            pltpu.VMEM((NZ, ROWS, COLS), BF),
            pltpu.VMEM((NZ, ROWS, COLS), BF),
            pltpu.VMEM((NZ, ROWS, COLS), BF),
            pltpu.VMEM((WIDTH, COLS), BF),
            pltpu.VMEM((WIDTH, COLS), BF),
            pltpu.VMEM((WIDTH, COLS), BF),
            pltpu.VMEM((NTP, ROWS, COLS), F32),
            pltpu.VMEM((NTP, ROWS, COLS), F32),
            pltpu.VMEM((NZ, 8, HEAD), F32),
            pltpu.VMEM((NY, 8, HEAD), F32),
            pltpu.VMEM((NTP, 8, HEAD), F32),
            dma((NY, NZ)),
            dma((NY, NZ)),
            dma((NZ,)),
            dma((NZ,)),
            dma((NZ,)),
            dma((NZ,)),
            *spread,
            *spread,
            *spread,
            dma((NZ,)),
            dma((NZ,)),
            dma((NY,)),
            dma((NY,)),
            dma((NTP,)),
            dma((NTP,)),
            dma((NTP,)),
            dma((NTP,)),
        ],
        compiler_params=pltpu.CompilerParams(collective_id=0, has_side_effects=True),
        name="fused",
    )(
        cotangent,
        values_first,
        values_second,
        head_lambda,
        out_gain.reshape(1, HEAD),
        weight,
        left_stat,
        right_stat,
        left_root,
        right_root,
    )


def solution(mesh):
    finer = Mesh(mesh.devices.reshape(NZ, NY, NX, NC), ("fs_0", "fs_1", "tp_0", "tp_1"))
    in_specs = (
        P(FS, None),
        P(FS, TP),
        P(FS, TP),
        P(TP),
        P(),
        P(FS, TP),
        P(FS, TP),
        P(TP, None, None),
        P(FS, None),
        P(TP, None, None),
    )
    out_specs = (P(FS, TP), P(FS, TP), P(None, TP), P(FS, TP), P(TP, None, None))
    return jax.shard_map(
        shards, mesh=finer, in_specs=in_specs, out_specs=out_specs, check_vma=False
    )
```

time: 360 us -> 89.9 us (0.25)
  the two profiles are of different devices: /device:TPU:2 before, /device:TPU:1 now
where the time goes in v1:
time: 89.9 us; the launch traced here: 89.7 us
  Pallas kernels  83.5 us (93%)
  local copies, waits for them, and re-layouts  5.57 us (6%)
    pallas_call x1, Pallas kernels, shards(): pl.pallas_call(kernel, out_shape=(jax.ShapeDtypeStruct((ROWS, COLS), F32)...  83.5 us
    unnamed x11, local copies, waits for them, and re-layouts  5.57 us

profile of v1, /device:TPU:1, one launch (start us, length us, event | category | flops | bytes accessed | tf_op | source)
XLA Modules:
  0.0 89.7 jit_solution(16557053580351334352)
XLA Ops:
  0.6 83.5 %fused.1 = (f32[32,256]{1,0:T(8,128)}, f32[32,256]{1,0:T(8,128)}, bf16[2048,256]{1,0:T(8,128)(2,1)}, f32[32,256]{1,0:T(8,128)}, f32[2,128,128]{2,1,0:T(8,128)}) custom-call(bf16[128,2048]{1,0:T(8,128)(2,1)} %cot.1, bf16[128,256]{1,0:T(8,128)(2,1)} %first.1, bf16[128,256]{1,0:T(8,128)(2,1)} %second.1, f32[2]{0:T(128)} %lam.1, f32[1,128]{1,0:T(1,128)} %bitcast.1, ...), custom_call_target="tpu_custom_call" | custom-call | tf_op jit(solution)/shard_map/fused/pallas_call | solution.py:413
  84.1 0.0 copy-start.2
  84.1 1.4 %copy.20 = f32[32,256]{1,0:T(8,128)} copy(f32[32,256]{1,0:T(8,128)} %get-tuple-element.10) | data formatting | bytes 65536
  85.5 0.0 copy-done.2
  85.5 0.6 copy.21
  86.1 0.0 copy-start.1
  86.1 0.0 copy-start
  86.1 2.3 %copy.22 = bf16[2048,256]{1,0:T(8,128)(2,1)} copy(bf16[2048,256]{1,0:T(8,128)(2,1)} %get-tuple-element.12) | data formatting | bytes 2097152
  88.4 0.0 copy-done.1
  88.4 0.6 copy.23
  89.0 0.0 copy-done
  89.1 0.7 copy.24
Async XLA Ops:
  84.1 1.4 %copy-start.2 = (f32[32,256]{1,0:T(8,128)S(1)}, f32[32,256]{1,0:T(8,128)}, u32[]{:S(2)}) copy-start(f32[32,256]{1,0:T(8,128)} %get-tuple-element.11) | copy-start | bytes 98308
  86.1 2.3 %copy-start.1 = (f32[32,256]{1,0:T(8,128)S(1)}, f32[32,256]{1,0:T(8,128)}, u32[]{:S(2)}) copy-start(f32[32,256]{1,0:T(8,128)} %get-tuple-element.13) | copy-start | bytes 98308
  86.1 2.9 %copy-start = (f32[2,128,128]{2,1,0:T(8,128)S(1)}, f32[2,128,128]{2,1,0:T(8,128)}, u32[]{:S(2)}) copy-start(f32[2,128,128]{2,1,0:T(8,128)} %get-tuple-element.14) | copy-start | bytes 393220

commit v2 on v1

v2 whole, which is shorter than its diff:
```python
import jax
import jax.numpy as jnp
from jax import lax
from jax.experimental import pallas as pl
from jax.experimental.pallas import tpu as pltpu
from jax.sharding import Mesh
from jax.sharding import PartitionSpec as P

TP = ("tp_0", "tp_1")
FS = ("fs_0", "fs_1")
NZ, NY, NX, NC = 16, 4, 4, 2
NTP = NX * NC
ROWS = 32
COLS = 256
HEAD = 128
WIDTH = 2048
REACH = 4
ORDER = (8, 7, 9, 6, 10, 5, 11, 4, 12, 3, 13, 2, 14, 1, 15)
UP, DOWN = (8, 7, 6), (9, 10)
DIRECT = (1, 15, 2, 14, 3, 13, 4, 12, 5, 11)
NEAR = (1, 15, 2, 14, 3, 13)
FAR = (5, 11, 6, 10, 7, 9, 8)

epsilon = 1e-06
decay_rate = 0.9
learn_rate = 0.01
output_scale = 0.2

BF = jnp.bfloat16
F32 = jnp.float32


def rows_of(z, y):
    return pl.ds(pl.multiple_of(z * (NY * ROWS) + y * ROWS, ROWS), ROWS)


def around(position, step, size):
    return lax.rem(position + (step % size), size)


def send(src, dst, send_sem, recv_sem, device):
    return pltpu.make_async_remote_copy(
        src_ref=src,
        dst_ref=dst,
        send_sem=send_sem,
        recv_sem=recv_sem,
        device_id=device,
        device_id_type=pl.DeviceIdType.MESH,
    )


class Spread:
    def __init__(self, buf, sems, at, slow=()):
        self.buf = buf
        self.zs, self.zr, self.ys, self.yr, self.ya = sems
        self.at = at
        self.slow = slow

    def block(self, step):
        z, y, x, c = self.at
        return self.buf.at[rows_of(around(z, -step, NZ), y)]

    def launch(self, step, reaches, down):
        z, y, x, c = self.at
        block = self.block(step)
        for reach in reaches:
            there = around(z, -reach if down else reach, NZ)
            arrives = (step - reach if down else step + reach) % NZ
            send(block, block, self.zs, self.zr.at[arrives], (there, y, x, c)).start()

    def begin(self):
        for reach in (1, 4, 2, 3):
            self.launch(0, (reach,), False)
            self.launch(0, (reach,), True)

    def wait(self, step):
        block = self.block(step)
        send(block, block, self.zs, self.zr.at[step], self.at).wait_recv()

    def relay(self):
        for reach in (1, 2, 3, 4):
            self.launch(4, (reach,), False)
            if reach < 4:
                self.launch(12, (reach,), True)

    def to_y(self, block, far, sem):
        z, y, x, c = self.at
        send(block, block, self.ys, sem, (z, around(y, far, NY), x, c)).start()

    def across(self, step):
        block = self.block(step)
        if step in self.slow:
            onward = 3 if step % 2 else 1
            self.to_y(block, onward, self.ya.at[step])
            self.to_y(block, NY - onward, self.yr)
        else:
            for far in (2, 1, 3):
                self.to_y(block, far, self.yr)

    def onward(self, step):
        z, y, x, c = self.at
        far = 3 if step % 2 else 1
        block = self.buf.at[rows_of(around(z, -step, NZ), around(y, -far, NY))]
        send(block, block, self.ys, self.ya.at[step], self.at).wait_recv()
        self.to_y(block, far, self.yr)

    def wait_across(self):
        every = self.buf.at[pl.ds(0, (NZ * (NY - 1) - len(self.slow)) * ROWS)]
        send(every, every, self.ys, self.yr, self.at).wait_recv()

    def drain(self):
        every = self.buf.at[pl.ds(0, NZ * (NY - 1) * ROWS)]
        send(every, every, self.ys, self.yr, self.at).wait_send()
        every = self.buf.at[pl.ds(0, (NZ - 1) * ROWS)]
        send(every, every, self.zs, self.zr.at[0], self.at).wait_send()


def kernel(
    cot_hbm,
    first_hbm,
    second_hbm,
    gain_hbm,
    weight_hbm,
    left_stat_hbm,
    right_stat_hbm,
    left_root_hbm,
    right_root_hbm,
    lam_hbm,
    update_step,
    new_weight,
    new_copy,
    new_left_stat,
    new_right_stat,
    cot,
    first,
    second,
    gain,
    weight,
    left_stat,
    right_stat,
    left_root,
    right_root,
    lam,
    load_sem,
    head_out,
    partial,
    partial_half,
    from_y,
    to_z,
    from_up,
    from_down,
    from_z,
    held_weight,
    portion,
    held_step,
    stat_out,
    stat_in,
    scal_s,
    scal_z,
    rys,
    ryr,
    rzs,
    rzr,
    rup,
    rdown,
    wzs,
    wzr,
    wys,
    wyr,
    wya,
    gzs,
    gzr,
    gys,
    gyr,
    pzs,
    pzr,
    pys,
    pyr,
    sss,
    ssr,
    szs,
    szr,
    lts,
    ltr,
):
    z, y, x, c = (lax.axis_index(a) for a in ("fs_0", "fs_1", "tp_0", "tp_1"))
    at = (z, y, x, c)
    me = x * NC + c

    def z_device(step):
        return (around(z, step, NZ), y, x, c)

    def y_device(step):
        return (z, around(y, step, NY), x, c)

    def t_index(step):
        return around(me, step, NTP)

    def plane_device(up, step):
        other = t_index(step)
        return (z, around(y, up, NY), other // NC, lax.rem(other, NC))

    loads = [
        pltpu.make_async_copy(source, there, load_sem.at[k])
        for k, (source, there) in enumerate(
            (
                (first_hbm, first),
                (second_hbm, second),
                (gain_hbm, gain),
                (lam_hbm, lam),
                (cot_hbm, cot),
                (weight_hbm, weight),
                (left_root_hbm, left_root),
                (right_root_hbm, right_root),
                (left_stat_hbm, left_stat),
                (right_stat_hbm, right_stat),
            )
        )
    ]
    for load in loads:
        load.start()
    barrier = pltpu.get_barrier_semaphore()
    plane = [(up, step) for up in range(NY) for step in range(NTP) if up or step]
    peers = [z_device(s) for s in DIRECT] + [y_device(s) for s in range(1, NY)]
    peers += [plane_device(0, s) for s in range(1, NTP)]
    for peer in peers:
        pl.semaphore_signal(barrier, inc=1, device_id=peer, device_id_type=pl.DeviceIdType.MESH)

    for load in loads[:4]:
        load.wait()
    for h in range(COLS // HEAD):
        lanes = slice(h * HEAD, (h + 1) * HEAD)
        difference = first[:, lanes].astype(F32) - lam[h] * second[:, lanes].astype(F32)
        mean = jnp.mean(difference * difference, axis=-1, keepdims=True)
        scaled = difference * lax.rsqrt(mean + epsilon) * gain[...] * output_scale
        head_out[:, lanes] = scaled.astype(BF)

    def chunk(step):
        zz = around(z, step, NZ)
        rows = pl.ds(pl.multiple_of(zz * HEAD, HEAD), HEAD)
        block = lax.dot_general(
            cot[:, rows], head_out[...], (((0,), (0,)), ((), ())), preferred_element_type=F32
        )
        partial[rows] = block
        partial_half[rows] = block.astype(BF)

    def chunk_out(step):
        zz = around(z, step, NZ)
        for far in (2, 1, 3):
            send(
                partial_half.at[rows_of(zz, around(y, far, NY))],
                from_y.at[step, far - 1],
                rys,
                ryr.at[step],
                y_device(far),
            ).start()

    loads[4].wait()
    for step in ORDER[:7]:
        chunk(step)
    loads[5].wait()
    held_weight[rows_of(z, y)] = weight[...].astype(BF)

    pl.semaphore_wait(barrier, len(peers))

    for step in ORDER[:7]:
        chunk_out(step)
    weights = Spread(held_weight, (wzs, wzr, wys, wyr, wya), at, range(NZ))
    weights.begin()
    for step in (*ORDER[7:], 0):
        chunk(step)
        chunk_out(step)

    def summed(step):
        every = from_y.at[step]
        send(every, every, rys, ryr.at[step], at).wait_recv()
        total = partial[rows_of(around(z, step, NZ), y)]
        for far in range(NY - 1):
            total = total + from_y[step, far].astype(F32)
        return total

    slot = {step: k for k, step in enumerate(DIRECT)}
    for step in ORDER:
        if step in (4, 12):
            continue
        to_z[step - 1] = summed(step).astype(BF)
        if step in UP:
            copy = send(to_z.at[step - 1], from_up.at[UP.index(step)], rzs, rup, z_device(step - REACH))
        elif step in DOWN:
            copy = send(to_z.at[step - 1], from_down.at[DOWN.index(step)], rzs, rdown, z_device(step + REACH))
        else:
            copy = send(to_z.at[step - 1], from_z.at[slot[step]], rzs, rzr, z_device(step))
        copy.start()
        if step == 13:
            for far, given, sem in ((4, from_up, rup), (12, from_down, rdown)):
                total = summed(far)
                send(given, given, rzs, sem, at).wait_recv()
                for k in range(given.shape[0]):
                    total = total + given[k].astype(F32)
                to_z[far - 1] = total.astype(BF)
                send(to_z.at[far - 1], from_z.at[slot[far]], rzs, rzr, z_device(far)).start()
    own = summed(0)
    weights.across(0)
    for step in (*NEAR, 4, 12):
        weights.wait(step)
    weights.relay()
    for step in (*NEAR, 4, 12):
        weights.across(step)
    for load in loads[6:]:
        load.wait()
    send(from_z, from_z, rzs, rzr, at).wait_recv()
    for k in range(len(DIRECT)):
        own = own + from_z[k].astype(F32)

    own_half = own.astype(BF)
    portion[rows_of(z, y)] = own_half
    grads = Spread(portion, (gzs, gzr, gys, gyr, None), at)
    grads.begin()
    grads.across(0)
    grad_square = jnp.sum(own * own, axis=(0, 1), keepdims=True)
    for step in NEAR:
        grads.wait(step)
        grads.across(step)
    grads.wait(4)
    grads.wait(12)
    grads.relay()
    grads.across(4)
    grads.across(12)
    for step in FAR:
        weights.wait(step)
        weights.across(step)
    for step in FAR:
        grads.wait(step)
        grads.across(step)
    grads.wait_across()

    left_half = jnp.dot(left_root[...], portion[...], preferred_element_type=F32).astype(BF)
    steps = [
        jnp.dot(left_half[:, h * HEAD : (h + 1) * HEAD], right_root[h], preferred_element_type=F32)
        for h in range(COLS // HEAD)
    ]
    precond = jnp.concatenate(steps, axis=1)
    held_step[rows_of(z, y)] = precond.astype(BF)
    places = Spread(held_step, (pzs, pzr, pys, pyr, None), at)
    step_square = jnp.sum(precond * precond, axis=(0, 1), keepdims=True)
    low = lax.broadcasted_iota(jnp.int32, (1, HEAD), 1) < HEAD // 2
    scal_z[z] = jnp.where(low, step_square, grad_square)
    places.begin()
    for step in ORDER:
        send(scal_z.at[z], scal_z.at[z], szs, szr, z_device(step)).start()
    places.across(0)
    for j in range(NTP):
        stat_out[j] = lax.dot_general(
            own_half,
            portion[j * COLS : (j + 1) * COLS],
            (((1,), (1,)), ((), ())),
            preferred_element_type=F32,
        )
    for far in range(1, NTP):
        send(stat_out.at[t_index(far)], stat_in.at[far - 1], lts, ltr, plane_device(0, far)).start()
    for h in range(COLS // HEAD):
        lanes = slice(h * HEAD, (h + 1) * HEAD)
        product = lax.dot_general(
            portion[:, lanes], portion[:, lanes], (((0,), (0,)), ((), ())), preferred_element_type=F32
        )
        new_right_stat[h] = decay_rate * right_stat[h] + (1.0 - decay_rate) / WIDTH * product

    for step in range(NZ):
        weights.onward(step)
    for step in NEAR:
        places.wait(step)
        places.across(step)
    places.wait(4)
    places.wait(12)
    places.relay()
    places.across(4)
    places.across(12)
    send(stat_in, stat_in, lts, ltr, at).wait_recv()
    stat = stat_out[me]
    for far in range(NTP - 1):
        stat = stat + stat_in[far]
    new_left_stat[...] = decay_rate * left_stat[...] + (1.0 - decay_rate) / WIDTH * stat
    for step in FAR[:2]:
        places.wait(step)
        places.across(step)
    every = scal_z.at[pl.ds(0, NZ - 1)]
    send(every, every, szs, szr, at).wait_recv()
    total = scal_z[0]
    for k in range(1, NZ):
        total = total + scal_z[k]
    mine = y * NTP + me
    scal_s[mine] = total
    for up, step in plane:
        send(scal_s.at[mine], scal_s.at[mine], sss, ssr, plane_device(up, step)).start()
    for step in FAR[2:]:
        places.wait(step)
        places.across(step)
    every = scal_s.at[pl.ds(0, NY * NTP - 1)]
    send(every, every, sss, ssr, at).wait_recv()
    total = scal_s[0]
    for k in range(1, NY * NTP):
        total = total + scal_s[k]
    factor = jnp.sqrt((total[:, HEAD // 2 : HEAD // 2 + 1] + epsilon) / (total[:, 0:1] + epsilon))

    step_own = factor * precond
    update_step[...] = step_own
    new_weight[...] = weight[...] - learn_rate * step_own
    weights.wait_across()
    places.wait_across()
    scale = learn_rate * factor
    for k in range(NZ):
        rows = pl.ds(k * HEAD, HEAD)
        new_copy[rows] = (held_weight[rows].astype(F32) - scale * held_step[rows].astype(F32)).astype(BF)

    every = partial_half.at[pl.ds(0, NZ * (NY - 1) * ROWS)]
    send(every, every, rys, ryr.at[0], at).wait_send()
    send(to_z, to_z, rzs, rzr, at).wait_send()
    every = scal_s.at[pl.ds(0, NY * NTP - 1)]
    send(every, every, sss, ssr, at).wait_send()
    every = scal_z.at[pl.ds(0, NZ - 1)]
    send(every, every, szs, szr, at).wait_send()
    send(stat_in, stat_in, lts, ltr, at).wait_send()
    for spread in (weights, grads, places):
        spread.drain()


def store(*refs):
    given, out, sem = refs[:5], refs[5:10], refs[10]
    copies = [pltpu.make_async_copy(a, b, sem.at[k]) for k, (a, b) in enumerate(zip(given, out))]
    for copy in copies:
        copy.start()
    for copy in copies:
        copy.wait()


def shards(
    cotangent,
    values_first,
    values_second,
    head_lambda,
    out_gain,
    weight,
    left_stat,
    right_stat,
    left_root,
    right_root,
):
    vmem = pl.BlockSpec(memory_space=pltpu.VMEM)
    anywhere = pl.BlockSpec(memory_space=pl.ANY)
    dma = pltpu.SemaphoreType.DMA
    spread = [dma, dma((NZ,)), dma, dma]
    given = (
        cotangent,
        values_first,
        values_second,
        out_gain.reshape(1, HEAD),
        weight,
        left_stat,
        right_stat,
        left_root,
        right_root,
        head_lambda,
    )
    results = (
        jax.ShapeDtypeStruct((ROWS, COLS), F32),
        jax.ShapeDtypeStruct((ROWS, COLS), F32),
        jax.ShapeDtypeStruct((WIDTH, COLS), BF),
        jax.ShapeDtypeStruct((ROWS, COLS), F32),
        jax.ShapeDtypeStruct((COLS // HEAD, HEAD, HEAD), F32),
    )
    outs = pl.pallas_call(
        kernel,
        out_shape=results,
        in_specs=[pl.BlockSpec(memory_space=pltpu.HBM)] * 10,
        out_specs=[vmem] * 5,
        scratch_shapes=[
            *[pltpu.VMEM(a.shape, a.dtype) for a in given[:9]],
            pltpu.SMEM(head_lambda.shape, F32),
            dma((10,)),
            pltpu.VMEM((128, COLS), BF),
            pltpu.VMEM((WIDTH, COLS), F32),
            pltpu.VMEM((WIDTH, COLS), BF),
            pltpu.VMEM((NZ, NY - 1, ROWS, COLS), BF),
            pltpu.VMEM((NZ - 1, ROWS, COLS), BF),
            pltpu.VMEM((len(UP), ROWS, COLS), BF),
            pltpu.VMEM((len(DOWN), ROWS, COLS), BF),
            pltpu.VMEM((len(DIRECT), ROWS, COLS), BF),
            pltpu.VMEM((WIDTH, COLS), BF),
            pltpu.VMEM((WIDTH, COLS), BF),
            pltpu.VMEM((WIDTH, COLS), BF),
            pltpu.VMEM((NTP, ROWS, COLS), F32),
            pltpu.VMEM((NTP - 1, ROWS, COLS), F32),
            pltpu.VMEM((NY * NTP, 1, HEAD), F32),
            pltpu.VMEM((NZ, 1, HEAD), F32),
            dma,
            dma((NZ,)),
            dma,
            dma,
            dma,
            dma,
            *spread,
            dma((NZ,)),
            *spread,
            *spread,
            dma,
            dma,
            dma,
            dma,
            dma,
            dma,
        ],
        compiler_params=pltpu.CompilerParams(
            collective_id=0, has_side_effects=True, vmem_limit_bytes=28 * 2**20
        ),
        name="fused",
    )(*[pltpu.with_memory_space_constraint(a, pltpu.HBM) for a in given])
    return pl.pallas_call(
        store,
        out_shape=results,
        in_specs=[vmem] * 5,
        out_specs=[anywhere] * 5,
        scratch_shapes=[dma((5,))],
        compiler_params=pltpu.CompilerParams(vmem_limit_bytes=8 * 2**20),
        name="store",
    )(*outs)


def solution(mesh):
    finer = Mesh(mesh.devices.reshape(NZ, NY, NX, NC), ("fs_0", "fs_1", "tp_0", "tp_1"))
    in_specs = (
        P(FS, None),
        P(FS, TP),
        P(FS, TP),
        P(TP),
        P(),
        P(FS, TP),
        P(FS, TP),
        P(TP, None, None),
        P(FS, None),
        P(TP, None, None),
    )
    out_specs = (P(FS, TP), P(FS, TP), P(None, TP), P(FS, TP), P(TP, None, None))
    return jax.shard_map(
        shards, mesh=finer, in_specs=in_specs, out_specs=out_specs, check_vma=False
    )
```

time: 89.9 us -> 69.1 us (0.77)
  the two profiles are of different devices: /device:TPU:1 before, /device:TPU:2 now
where the time goes in v2:
time: 69.1 us; the launch traced here: 68.9 us
  Pallas kernels  68.3 us (99%)
    pallas_call x1, Pallas kernels, shards(): pl.pallas_call(kernel, out_shape=results, in_specs=[pl.BlockSpec(memory_s...  67.2 us

profile of v2, /device:TPU:2, one launch (start us, length us, event | category | flops | bytes accessed | tf_op | source)
XLA Modules:
  0.0 68.9 jit_solution(16948172868236760643)
XLA Ops:
  0.6 67.2 %fused.1 = (f32[32,256]{1,0:T(8,128)S(1)}, f32[32,256]{1,0:T(8,128)S(1)}, bf16[2048,256]{1,0:T(8,128)(2,1)S(1)}, f32[32,256]{1,0:T(8,128)S(1)}, f32[2,128,128]{2,1,0:T(8,128)S(1)}) custom-call(bf16[128,2048]{1,0:T(8,128)(2,1)} %cot_hbm.1, bf16[128,256]{1,0:T(8,128)(2,1)} %first_hbm.1, bf16[128,256]{1,0:T(8,128)(2,1)} %second_hbm.1, f32[1,128]{1,0:T(1,128)} %bitcast.1, ...), custom_call_target="tpu_custom_call" | custom-call | tf_op jit(solution)/shard_map/fused/pallas_call | solution.py:471
  67.9 1.1 %store.1 = (f32[32,256]{1,0:T(8,128)}, f32[32,256]{1,0:T(8,128)}, bf16[2048,256]{1,0:T(8,128)(2,1)}, f32[32,256]{1,0:T(8,128)}, f32[2,128,128]{2,1,0:T(8,128)}) custom-call(f32[32,256]{1,0:T(8,128)S(1)} %get-tuple-element.10.refs_0_, f32[32,256]{1,0:T(8,128)S(1)} %get-tuple-element.11.refs_1_, bf16[2048,256]{1,0:T(8,128)(2,1)S(1)} %get-tuple-element.12.refs_2_, ...), custom_call_target="tpu_custom_call" | custom-call | tf_op jit(solution)/shard_map/store/pallas_call | solution.py:517

commit v3 on v0

v3 whole, which is shorter than its diff:
```python
import jax
import jax.numpy as jnp
from jax import lax
from jax.experimental import pallas as pl
from jax.experimental.pallas import tpu as pltpu
from jax.sharding import Mesh
from jax.sharding import PartitionSpec as P

TP = ("tp_0", "tp_1")
FS = ("fs_0", "fs_1")
NZ, NY, NX, NC = 16, 4, 4, 2
NTP = NX * NC
ROWS = 32
COLS = 256
HEAD = 128
WIDTH = 2048
REACH = 4
HEADS = COLS // HEAD
ORDER = (8, 7, 9, 6, 10, 5, 11, 4, 12, 3, 13, 2, 14, 1, 15, 0)
BATCH = ((8, 7), (9, 6), (10,), (5, 11), (4, 12), (3, 13), (2, 14), (1, 15), (0,))
UP, DOWN = (8, 7, 6), (9, 10)
DIRECT = (1, 15, 2, 14, 3, 13, 4, 12, 5, 11)
NEAR = ((1, 15), (2, 14), (3, 13))
MID = ((4,), (12,))
FAR = ((5, 11), (6, 10), (7, 9), (8,))
GROUPS = NEAR + MID + FAR
GROUP_OF = {step: k for k, group in enumerate(GROUPS) for step in group}

epsilon = 1e-06
decay_rate = 0.9
learn_rate = 0.01
output_scale = 0.2

BF = jnp.bfloat16
F32 = jnp.float32


def rows_of(z, y):
    return pl.ds(pl.multiple_of(z * (NY * ROWS) + y * ROWS, ROWS), ROWS)


def around(position, step, size):
    return lax.rem(position + (step % size), size)


def send(src, dst, send_sem, recv_sem, device):
    return pltpu.make_async_remote_copy(
        src_ref=src,
        dst_ref=dst,
        send_sem=send_sem,
        recv_sem=recv_sem,
        device_id=device,
        device_id_type=pl.DeviceIdType.MESH,
    )


class Spread:
    def __init__(self, buf, sems, at, slow=False):
        self.buf = buf
        self.zs, self.zr, self.ys, self.yr, self.ya = sems
        self.at = at
        self.slow = slow

    def block(self, step):
        z, y, x, c = self.at
        return self.buf.at[rows_of(around(z, -step, NZ), y)]

    def whole(self, blocks):
        return self.buf.at[pl.ds(0, blocks * ROWS)]

    def launch(self, step, reach, down):
        z, y, x, c = self.at
        block = self.block(step)
        there = around(z, -reach if down else reach, NZ)
        arrives = (step - reach if down else step + reach) % NZ
        send(block, block, self.zs, self.zr.at[GROUP_OF[arrives]], (there, y, x, c)).start()

    def begin(self):
        for reach in (1, 4, 2, 3):
            self.launch(0, reach, False)
            self.launch(0, reach, True)

    def wait(self, group):
        every = self.whole(len(group))
        send(every, every, self.zs, self.zr.at[GROUP_OF[group[0]]], self.at).wait_recv()

    def relay(self):
        for reach in (1, 2, 3, 4):
            self.launch(4, reach, False)
            if reach < 4:
                self.launch(12, reach, True)

    def to_y(self, block, far, sem):
        z, y, x, c = self.at
        send(block, block, self.ys, sem, (z, around(y, far, NY), x, c)).start()

    def across(self, group):
        for step in group:
            block = self.block(step)
            if self.slow:
                onward = 3 if step % 2 else 1
                self.to_y(block, onward, self.ya)
                self.to_y(block, NY - onward, self.yr)
            else:
                for far in (2, 1, 3):
                    self.to_y(block, far, self.yr)

    def take(self, groups):
        for group in groups:
            self.wait(group)
            self.across(group)

    def onward(self):
        z, y, x, c = self.at
        every = self.whole(NZ)
        send(every, every, self.ys, self.ya, self.at).wait_recv()
        for step in range(NZ):
            far = 3 if step % 2 else 1
            block = self.buf.at[rows_of(around(z, -step, NZ), around(y, -far, NY))]
            self.to_y(block, far, self.yr)

    def wait_across(self):
        every = self.whole(NZ * (2 if self.slow else 3))
        send(every, every, self.ys, self.yr, self.at).wait_recv()

    def drain(self):
        every = self.whole(NZ * (NY - 1))
        send(every, every, self.ys, self.yr, self.at).wait_send()
        every = self.whole(NZ - 1)
        send(every, every, self.zs, self.zr.at[0], self.at).wait_send()


def kernel(*refs):
    refs = list(refs)

    def grab(count):
        taken = refs[:count]
        del refs[:count]
        return taken

    sources = grab(10)
    update_step, new_weight, new_copy, new_left_stat, new_right_stat = grab(5)
    local = grab(10)
    first, second, gain, lam, cot, weight, left_root, right_root, left_stat, right_stat = local
    (load_sem,) = grab(1)
    head_out, partial = grab(2)
    partial_half, from_y, to_z, from_up, from_down, from_z = (grab(HEADS) for _ in range(6))
    (held_weight,) = grab(1)
    portion, held_step = grab(HEADS), grab(HEADS)
    stat_out, stat_in, scal_s, scal_z = grab(4)
    rys, ryr, rzs, rzr, rup, rdown = (grab(HEADS) for _ in range(6))
    wsems = grab(5)
    gsems = [[*grab(4), None] for _ in range(HEADS)]
    psems = [[*grab(4), None] for _ in range(HEADS)]
    sss, ssr, szs, szr, lts, ltr = grab(6)

    z, y, x, c = (lax.axis_index(a) for a in ("fs_0", "fs_1", "tp_0", "tp_1"))
    at = (z, y, x, c)
    me = x * NC + c
    both = range(HEADS)
    lanes = [slice(h * HEAD, (h + 1) * HEAD) for h in both]

    def z_device(step):
        return (around(z, step, NZ), y, x, c)

    def y_device(step):
        return (z, around(y, step, NY), x, c)

    def t_index(step):
        return around(me, step, NTP)

    def t_device(step):
        other = t_index(step)
        return (z, y, other // NC, lax.rem(other, NC))

    loads = [pltpu.make_async_copy(a, b, load_sem.at[k]) for k, (a, b) in enumerate(zip(sources, local))]
    for load in loads:
        load.start()
    barrier = pltpu.get_barrier_semaphore()
    peers = [z_device(s) for s in DIRECT] + [y_device(s) for s in range(1, NY)]
    peers += [t_device(s) for s in range(1, NTP)]
    for peer in peers:
        pl.semaphore_signal(barrier, inc=1, device_id=peer, device_id_type=pl.DeviceIdType.MESH)

    for load in loads[:4]:
        load.wait()
    for h in both:
        difference = first[:, lanes[h]].astype(F32) - lam[h] * second[:, lanes[h]].astype(F32)
        mean = jnp.mean(difference * difference, axis=-1, keepdims=True)
        scaled = difference * lax.rsqrt(mean + epsilon) * gain[...] * output_scale
        head_out[:, lanes[h]] = scaled.astype(BF)

    def chunk(step):
        zz = around(z, step, NZ)
        rows = pl.ds(pl.multiple_of(zz * HEAD, HEAD), HEAD)
        block = lax.dot_general(
            cot[:, rows], head_out[...], (((0,), (0,)), ((), ())), preferred_element_type=F32
        )
        partial[rows] = block
        for h in both:
            partial_half[h][rows] = block[:, lanes[h]].astype(BF)

    batch_of = {step: k for k, group in enumerate(BATCH) for step in group}
    spot = {step: k for k, step in enumerate(step for group in BATCH for step in group)}

    def chunk_out(h, step):
        zz = around(z, step, NZ)
        for far in (2, 1, 3):
            send(
                partial_half[h].at[rows_of(zz, around(y, far, NY))],
                from_y[h].at[spot[step], far - 1],
                rys[h],
                ryr[h].at[batch_of[step]],
                y_device(far),
            ).start()

    loads[4].wait()
    for step in ORDER[:7]:
        chunk(step)
    loads[5].wait()
    held_weight[rows_of(z, y)] = weight[...].astype(BF)

    pl.semaphore_wait(barrier, len(peers))

    for h in both:
        for step in ORDER[:5]:
            chunk_out(h, step)
    weights = Spread(held_weight, wsems, at, True)
    weights.begin()
    for step in ORDER[5:7]:
        chunk_out(0, step)
    for step in ORDER[7:]:
        chunk(step)
        chunk_out(0, step)
    for step in ORDER[5:]:
        chunk_out(1, step)

    def arrive(h, group):
        block = from_y[h].at[pl.ds(spot[group[0]], len(group))]
        send(block, block, rys[h], ryr[h].at[batch_of[group[0]]], at).wait_recv()

    def summed(h, step):
        total = partial[rows_of(around(z, step, NZ), y), lanes[h]]
        for far in range(NY - 1):
            total = total + from_y[h][spot[step], far].astype(F32)
        return total

    slot = {step: k for k, step in enumerate(DIRECT)}

    def pass_on(h, groups):
        for group in groups:
            arrive(h, group)
            for step in group:
                out = to_z[h].at[step - 1]
                to_z[h][step - 1] = summed(h, step).astype(BF)
                if step in UP:
                    send(out, from_up[h].at[UP.index(step)], rzs[h], rup[h], z_device(step - REACH)).start()
                elif step in DOWN:
                    send(out, from_down[h].at[DOWN.index(step)], rzs[h], rdown[h], z_device(step + REACH)).start()
                else:
                    send(out, from_z[h].at[slot[step]], rzs[h], rzr[h], z_device(step)).start()

    def combine(h):
        arrive(h, BATCH[4])
        for far, given, sem in ((4, from_up[h], rup[h]), (12, from_down[h], rdown[h])):
            total = summed(h, far)
            send(given, given, rzs[h], sem, at).wait_recv()
            for k in range(given.shape[0]):
                total = total + given[k].astype(F32)
            to_z[h][far - 1] = total.astype(BF)
            send(to_z[h].at[far - 1], from_z[h].at[slot[far]], rzs[h], rzr[h], z_device(far)).start()

    def finish(h):
        arrive(h, BATCH[8])
        own = summed(h, 0)
        send(from_z[h], from_z[h], rzs[h], rzr[h], at).wait_recv()
        for k in range(len(DIRECT)):
            own = own + from_z[h][k].astype(F32)
        return own

    pass_on(0, BATCH[:3])
    pass_on(1, BATCH[:3])
    pass_on(0, BATCH[3:4])
    combine(0)
    pass_on(0, BATCH[5:8])
    pass_on(1, BATCH[3:4])
    combine(1)
    pass_on(1, BATCH[5:8])
    own, own_half, grads = [None] * HEADS, [None] * HEADS, [None] * HEADS

    def gather(h):
        own[h] = finish(h)
        own_half[h] = own[h].astype(BF)
        portion[h][rows_of(z, y)] = own_half[h]
        grads[h] = Spread(portion[h], gsems[h], at)
        grads[h].begin()
        grads[h].across((0,))

    gather(0)
    weights.across((0,))
    for group in NEAR + MID:
        weights.wait(group)
    for group in NEAR + MID:
        weights.across(group)
    for load in loads[6:]:
        load.wait()
    gather(1)
    grads[0].take(NEAR)
    for group in MID:
        grads[0].wait(group)
    grads[0].relay()
    for group in MID:
        grads[0].across(group)
    grads[1].take(NEAR)
    for group in MID:
        grads[1].wait(group)
    grads[1].relay()
    weights.relay()
    for group in MID:
        grads[1].across(group)
    grads[0].take(FAR)
    grads[1].take(FAR)

    precond, places = [None] * HEADS, [None] * HEADS

    def advance(h):
        left_half = jnp.dot(left_root[...], portion[h][...], preferred_element_type=F32).astype(BF)
        precond[h] = jnp.dot(left_half, right_root[h], preferred_element_type=F32)
        held_step[h][rows_of(z, y)] = precond[h].astype(BF)
        places[h] = Spread(held_step[h], psems[h], at)
        places[h].begin()
        places[h].across((0,))

    grads[0].wait_across()
    advance(0)
    weights.take(FAR)
    grads[1].wait_across()
    advance(1)
    squares = [jnp.sum(v * v, axis=(0, 1), keepdims=True) for v in (*precond, *own)]
    low = lax.broadcasted_iota(jnp.int32, (1, HEAD), 1) < HEAD // 2
    mine = z * NY + y
    scal_z[mine] = jnp.where(low, squares[0] + squares[1], squares[2] + squares[3])
    for step in ORDER:
        for up in (2, 1, 3, 0):
            if step or up:
                there = (around(z, step, NZ), around(y, up, NY), x, c)
                send(scal_z.at[mine], scal_z.at[mine], szs, szr, there).start()
    places[0].take(NEAR)
    for group in MID:
        places[0].wait(group)
    places[0].relay()
    for group in MID:
        places[0].across(group)

    contract = (((1,), (1,)), ((), ()))
    for j in range(NTP):
        rows = slice(j * COLS, (j + 1) * COLS)
        stat_out[j] = sum(
            lax.dot_general(own_half[h], portion[h][rows], contract, preferred_element_type=F32)
            for h in both
        )
    for far in range(1, NTP):
        send(stat_out.at[t_index(far)], stat_in.at[far - 1], lts, ltr, t_device(far)).start()
    for h in both:
        product = lax.dot_general(
            portion[h][...], portion[h][...], (((0,), (0,)), ((), ())), preferred_element_type=F32
        )
        new_right_stat[h] = decay_rate * right_stat[h] + (1.0 - decay_rate) / WIDTH * product
    weights.onward()
    places[1].take(NEAR)
    for group in MID:
        places[1].wait(group)
    places[1].relay()
    for group in MID:
        places[1].across(group)
    places[0].take(FAR)
    every = scal_z.at[pl.ds(0, NZ * NY - 1)]
    send(every, every, szs, szr, at).wait_recv()
    total = scal_z[0]
    for k in range(1, NZ * NY):
        total = total + scal_z[k]
    scal_s[me] = total
    for step in range(1, NTP):
        send(scal_s.at[me], scal_s.at[me], sss, ssr, t_device(step)).start()
    places[1].take(FAR)
    send(stat_in, stat_in, lts, ltr, at).wait_recv()
    stat = stat_out[me]
    for far in range(NTP - 1):
        stat = stat + stat_in[far]
    new_left_stat[...] = decay_rate * left_stat[...] + (1.0 - decay_rate) / WIDTH * stat
    every = scal_s.at[pl.ds(0, NTP - 1)]
    send(every, every, sss, ssr, at).wait_recv()
    total = scal_s[0]
    for k in range(1, NTP):
        total = total + scal_s[k]
    factor = jnp.sqrt((total[:, HEAD // 2 : HEAD // 2 + 1] + epsilon) / (total[:, 0:1] + epsilon))
    for h in both:
        step_own = factor * precond[h]
        update_step[:, lanes[h]] = step_own
        new_weight[:, lanes[h]] = weight[:, lanes[h]] - learn_rate * step_own
    weights.wait_across()
    scale = learn_rate * factor
    for h in both:
        places[h].wait_across()
        for k in range(NZ):
            rows = pl.ds(k * HEAD, HEAD)
            held = held_weight[rows, lanes[h]].astype(F32)
            new_copy[rows, lanes[h]] = (held - scale * held_step[h][rows].astype(F32)).astype(BF)

    for h in both:
        every = partial_half[h].at[pl.ds(0, NZ * (NY - 1) * ROWS)]
        send(every, every, rys[h], ryr[h].at[0], at).wait_send()
        send(to_z[h], to_z[h], rzs[h], rzr[h], at).wait_send()
    every = scal_s.at[pl.ds(0, NTP - 1)]
    send(every, every, sss, ssr, at).wait_send()
    every = scal_z.at[pl.ds(0, NZ * NY - 1)]
    send(every, every, szs, szr, at).wait_send()
    send(stat_in, stat_in, lts, ltr, at).wait_send()
    for spread in (weights, *grads, *places):
        spread.drain()


def store(*refs):
    given, out, sem = refs[:5], refs[5:10], refs[10]
    copies = [pltpu.make_async_copy(a, b, sem.at[k]) for k, (a, b) in enumerate(zip(given, out))]
    for copy in copies:
        copy.start()
    for copy in copies:
        copy.wait()


def shards(
    cotangent,
    values_first,
    values_second,
    head_lambda,
    out_gain,
    weight,
    left_stat,
    right_stat,
    left_root,
    right_root,
):
    vmem = pl.BlockSpec(memory_space=pltpu.VMEM)
    anywhere = pl.BlockSpec(memory_space=pl.ANY)
    dma = pltpu.SemaphoreType.DMA
    spread = [dma, dma((len(GROUPS),)), dma, dma]
    given = (
        values_first,
        values_second,
        out_gain.reshape(1, HEAD),
        head_lambda,
        cotangent,
        weight,
        left_root,
        right_root,
        left_stat,
        right_stat,
    )
    local = [pltpu.SMEM(a.shape, F32) if a is head_lambda else pltpu.VMEM(a.shape, a.dtype) for a in given]

    def per_head(*shape):
        return [pltpu.VMEM((*shape, HEAD), BF)] * HEADS

    results = (
        jax.ShapeDtypeStruct((ROWS, COLS), F32),
        jax.ShapeDtypeStruct((ROWS, COLS), F32),
        jax.ShapeDtypeStruct((WIDTH, COLS), BF),
        jax.ShapeDtypeStruct((ROWS, COLS), F32),
        jax.ShapeDtypeStruct((COLS // HEAD, HEAD, HEAD), F32),
    )
    outs = pl.pallas_call(
        kernel,
        out_shape=results,
        in_specs=[pl.BlockSpec(memory_space=pltpu.HBM)] * 10,
        out_specs=[vmem] * 5,
        scratch_shapes=[
            *local,
            dma((10,)),
            pltpu.VMEM((128, COLS), BF),
            pltpu.VMEM((WIDTH, COLS), F32),
            *per_head(WIDTH),
            *per_head(NZ, NY - 1, ROWS),
            *per_head(NZ - 1, ROWS),
            *per_head(len(UP), ROWS),
            *per_head(len(DOWN), ROWS),
            *per_head(len(DIRECT), ROWS),
            pltpu.VMEM((WIDTH, COLS), BF),
            *per_head(WIDTH),
            *per_head(WIDTH),
            pltpu.VMEM((NTP, ROWS, COLS), F32),
            pltpu.VMEM((NTP - 1, ROWS, COLS), F32),
            pltpu.VMEM((NTP, 1, HEAD), F32),
            pltpu.VMEM((NZ * NY, 1, HEAD), F32),
            *[dma] * HEADS,
            *[dma((len(BATCH),))] * HEADS,
            *[dma] * (4 * HEADS),
            *spread,
            dma,
            *spread * (2 * HEADS),
            *[dma] * 6,
        ],
        compiler_params=pltpu.CompilerParams(
            collective_id=0, has_side_effects=True, vmem_limit_bytes=28 * 2**20
        ),
        name="fused",
    )(*[pltpu.with_memory_space_constraint(a, pltpu.HBM) for a in given])
    return pl.pallas_call(
        store,
        out_shape=results,
        in_specs=[vmem] * 5,
        out_specs=[anywhere] * 5,
        scratch_shapes=[dma((5,))],
        compiler_params=pltpu.CompilerParams(vmem_limit_bytes=8 * 2**20),
        name="store",
    )(*outs)


def solution(mesh):
    finer = Mesh(mesh.devices.reshape(NZ, NY, NX, NC), ("fs_0", "fs_1", "tp_0", "tp_1"))
    in_specs = (
        P(FS, None),
        P(FS, TP),
        P(FS, TP),
        P(TP),
        P(),
        P(FS, TP),
        P(FS, TP),
        P(TP, None, None),
        P(FS, None),
        P(TP, None, None),
    )
    out_specs = (P(FS, TP), P(FS, TP), P(None, TP), P(FS, TP), P(TP, None, None))
    return jax.shard_map(
        shards, mesh=finer, in_specs=in_specs, out_specs=out_specs, check_vma=False
    )
```

time: 360 us -> 64.4 us (0.18)
  waiting for transfers between devices: 237 us -> 0 us
  blocking collectives: 79.3 us -> 0 us
  Pallas kernels: 0 us -> 63.6 us
  between operations: 15.2 us -> 0.64 us
  local copies, waits for them, and re-layouts: 11.4 us -> 0 us
  matrix products: 6.4 us -> 0 us
  starting transfers between devices: 5.83 us -> 0 us
  other arithmetic: 3.68 us -> 0 us
    all_gather x2 -> x0, waiting for transfers between devices: 119 us -> none  [gather_axes(): nearer = lax.all_gather(value, axes[-1], axis=dim, tiled=True)]
    reduce_scatter x2 -> x0, waiting for transfers between devices: 115 us -> none  [reduced_to_own(): pieces = lax.psum_scatter(pieces, axes[k], scatter_dimension=0, tiled=True)]
    pallas_call x0 -> x2, Pallas kernels: none -> 63.6 us  [the longest x1 62.5 us: shards(): pl.pallas_call(kernel, out_shape=results, in_specs=[pl.BlockSpec(memory_s...]
    psum x4 -> x0, blocking collectives: 53.8 us -> none  [by_axis(): return functools.reduce(lax.psum, axes, value)]
    all_gather x2 -> x0, blocking collectives: 25.5 us -> none  [gather_axes(): nearer = lax.all_gather(value, axes[-1], axis=dim, tiled=True)]
    dot_general x5 -> x0, matrix products: 6.4 us -> none  [the longest x1 1.63 us: shards(): lax.dot_general(grad_half, portion, contract_cols, preferred_element_type...]
    all_to_all x1 -> x0, starting transfers between devices: 5.67 us -> none  [summed_on_arrival(): lax.all_to_all(pieces, axis, split_axis=0, concat_axis=0, tiled=True)]
  transfers between devices with their start and end apart: 5 -> 0, of which waited for: 5 -> 0; matrix products, arithmetic and copies ran while one was open for 1% -> 0% of each run, Pallas kernels for 0% -> 0%
where the time goes in v3:
time: 64.4 us; the launch traced here: 64.2 us
  Pallas kernels  63.6 us (99%)
    pallas_call x1, Pallas kernels, shards(): pl.pallas_call(kernel, out_shape=results, in_specs=[pl.BlockSpec(memory_s...  62.5 us

profile of v3, /device:TPU:2, one launch (start us, length us, event | category | flops | bytes accessed | tf_op | source)
XLA Modules:
  0.0 64.2 jit_solution(16859434360046040225)
XLA Ops:
  0.6 62.5 %fused.1 = (f32[32,256]{1,0:T(8,128)S(1)}, f32[32,256]{1,0:T(8,128)S(1)}, bf16[2048,256]{1,0:T(8,128)(2,1)S(1)}, f32[32,256]{1,0:T(8,128)S(1)}, f32[2,128,128]{2,1,0:T(8,128)S(1)}) custom-call(bf16[128,256]{1,0:T(8,128)(2,1)} %refs_0_.1, bf16[128,256]{1,0:T(8,128)(2,1)} %refs_1_.1, f32[1,128]{1,0:T(1,128)} %bitcast.1, f32[2]{0:T(128)} %refs_3_.1, ...), custom_call_target="tpu_custom_call" | custom-call | tf_op jit(solution)/shard_map/fused/pallas_call | solution.py:472
  63.1 1.1 %store.1 = (f32[32,256]{1,0:T(8,128)}, f32[32,256]{1,0:T(8,128)}, bf16[2048,256]{1,0:T(8,128)(2,1)}, f32[32,256]{1,0:T(8,128)}, f32[2,128,128]{2,1,0:T(8,128)}) custom-call(f32[32,256]{1,0:T(8,128)S(1)} %get-tuple-element.10.refs_0_, f32[32,256]{1,0:T(8,128)S(1)} %get-tuple-element.11.refs_1_, bf16[2048,256]{1,0:T(8,128)(2,1)S(1)} %get-tuple-element.12.refs_2_, ...), custom_call_target="tpu_custom_call" | custom-call | tf_op jit(solution)/shard_map/store/pallas_call | solution.py:508

commit v4 on v3

--- a/solution.py
+++ b/solution.py
@@ -18,8 +18,8 @@
 HEADS = COLS // HEAD
 ORDER = (8, 7, 9, 6, 10, 5, 11, 4, 12, 3, 13, 2, 14, 1, 15, 0)
 BATCH = ((8, 7), (9, 6), (10,), (5, 11), (4, 12), (3, 13), (2, 14), (1, 15), (0,))
-UP, DOWN = (8, 7, 6), (9, 10)
-DIRECT = (1, 15, 2, 14, 3, 13, 4, 12, 5, 11)
+UP, DOWN = (8, 7, 6, 5), (9, 10, 11)
+DIRECT = (1, 15, 2, 14, 3, 13, 4, 12)
 NEAR = ((1, 15), (2, 14), (3, 13))
 MID = ((4,), (12,))
 FAR = ((5, 11), (6, 10), (7, 9), (8,))
@@ -223,16 +223,14 @@
     pl.semaphore_wait(barrier, len(peers))
 
     for h in both:
-        for step in ORDER[:5]:
+        for step in ORDER[:7]:
             chunk_out(h, step)
     weights = Spread(held_weight, wsems, at, True)
     weights.begin()
-    for step in ORDER[5:7]:
-        chunk_out(0, step)
     for step in ORDER[7:]:
         chunk(step)
         chunk_out(0, step)
-    for step in ORDER[5:]:
+    for step in ORDER[7:]:
         chunk_out(1, step)
 
     def arrive(h, group):
@@ -278,12 +276,10 @@
             own = own + from_z[h][k].astype(F32)
         return own
 
-    pass_on(0, BATCH[:3])
-    pass_on(1, BATCH[:3])
-    pass_on(0, BATCH[3:4])
+    pass_on(0, BATCH[:4])
+    pass_on(1, BATCH[:4])
     combine(0)
     pass_on(0, BATCH[5:8])
-    pass_on(1, BATCH[3:4])
     combine(1)
     pass_on(1, BATCH[5:8])
     own, own_half, grads = [None] * HEADS, [None] * HEADS, [None] * HEADS
@@ -323,9 +319,22 @@
 
     precond, places = [None] * HEADS, [None] * HEADS
 
+    def send_squares():
+        squares = [jnp.sum(v * v, axis=(0, 1), keepdims=True) for v in (*precond, *own)]
+        low = lax.broadcasted_iota(jnp.int32, (1, HEAD), 1) < HEAD // 2
+        mine = z * NY + y
+        scal_z[mine] = jnp.where(low, squares[0] + squares[1], squares[2] + squares[3])
+        for step in ORDER:
+            for up in (2, 1, 3, 0):
+                if step or up:
+                    there = (around(z, step, NZ), around(y, up, NY), x, c)
+                    send(scal_z.at[mine], scal_z.at[mine], szs, szr, there).start()
+
     def advance(h):
         left_half = jnp.dot(left_root[...], portion[h][...], preferred_element_type=F32).astype(BF)
         precond[h] = jnp.dot(left_half, right_root[h], preferred_element_type=F32)
+        if h == HEADS - 1:
+            send_squares()
         held_step[h][rows_of(z, y)] = precond[h].astype(BF)
         places[h] = Spread(held_step[h], psems[h], at)
         places[h].begin()
@@ -336,15 +345,6 @@
     weights.take(FAR)
     grads[1].wait_across()
     advance(1)
-    squares = [jnp.sum(v * v, axis=(0, 1), keepdims=True) for v in (*precond, *own)]
-    low = lax.broadcasted_iota(jnp.int32, (1, HEAD), 1) < HEAD // 2
-    mine = z * NY + y
-    scal_z[mine] = jnp.where(low, squares[0] + squares[1], squares[2] + squares[3])
-    for step in ORDER:
-        for up in (2, 1, 3, 0):
-            if step or up:
-                there = (around(z, step, NZ), around(y, up, NY), x, c)
-                send(scal_z.at[mine], scal_z.at[mine], szs, szr, there).start()
     places[0].take(NEAR)
     for group in MID:
         places[0].wait(group)
@@ -352,6 +352,13 @@
     for group in MID:
         places[0].across(group)
 
+    weights.onward()
+    places[1].take(NEAR)
+    for group in MID:
+        places[1].wait(group)
+    places[1].relay()
+    for group in MID:
+        places[1].across(group)
     contract = (((1,), (1,)), ((), ()))
     for j in range(NTP):
         rows = slice(j * COLS, (j + 1) * COLS)
@@ -366,13 +373,6 @@
             portion[h][...], portion[h][...], (((0,), (0,)), ((), ())), preferred_element_type=F32
         )
         new_right_stat[h] = decay_rate * right_stat[h] + (1.0 - decay_rate) / WIDTH * product
-    weights.onward()
-    places[1].take(NEAR)
-    for group in MID:
-        places[1].wait(group)
-    places[1].relay()
-    for group in MID:
-        places[1].across(group)
     places[0].take(FAR)
     every = scal_z.at[pl.ds(0, NZ * NY - 1)]
     send(every, every, szs, szr, at).wait_recv()

time: 64.4 us -> 63 us (0.978)
  Pallas kernels: 63.6 us -> 62.2 us
    pallas_call x1, Pallas kernels: 62.5 us -> 61.1 us  [shards(): pl.pallas_call(kernel, out_shape=results, in_specs=[pl.BlockSpec(memory_s...]
where the time goes in v4:
time: 63 us; the launch traced here: 62.9 us
  Pallas kernels  62.2 us (99%)
  between operations  0.64 us (1%)
    pallas_call x1, Pallas kernels, shards(): pl.pallas_call(kernel, out_shape=results, in_specs=[pl.BlockSpec(memory_s...  61.1 us

profile of v4, /device:TPU:2, one launch (start us, length us, event | category | flops | bytes accessed | tf_op | source)
XLA Modules:
  0.0 62.9 jit_solution(17681444027421503940)
XLA Ops:
  0.6 61.1 %fused.1 = (f32[32,256]{1,0:T(8,128)S(1)}, f32[32,256]{1,0:T(8,128)S(1)}, bf16[2048,256]{1,0:T(8,128)(2,1)S(1)}, f32[32,256]{1,0:T(8,128)S(1)}, f32[2,128,128]{2,1,0:T(8,128)S(1)}) custom-call(bf16[128,256]{1,0:T(8,128)(2,1)} %refs_0_.1, bf16[128,256]{1,0:T(8,128)(2,1)} %refs_1_.1, f32[1,128]{1,0:T(1,128)} %bitcast.1, f32[2]{0:T(128)} %refs_3_.1, ...), custom_call_target="tpu_custom_call" | custom-call | tf_op jit(solution)/shard_map/fused/pallas_call | solution.py:472
  61.8 1.1 %store.1 = (f32[32,256]{1,0:T(8,128)}, f32[32,256]{1,0:T(8,128)}, bf16[2048,256]{1,0:T(8,128)(2,1)}, f32[32,256]{1,0:T(8,128)}, f32[2,128,128]{2,1,0:T(8,128)}) custom-call(f32[32,256]{1,0:T(8,128)S(1)} %get-tuple-element.10.refs_0_, f32[32,256]{1,0:T(8,128)S(1)} %get-tuple-element.11.refs_1_, bf16[2048,256]{1,0:T(8,128)(2,1)S(1)} %get-tuple-element.12.refs_2_, ...), custom_call_target="tpu_custom_call" | custom-call | tf_op jit(solution)/shard_map/store/pallas_call | solution.py:508

commit v5 on v4

--- a/solution.py
+++ b/solution.py
@@ -173,15 +173,15 @@
         other = t_index(step)
         return (z, y, other // NC, lax.rem(other, NC))
 
-    loads = [pltpu.make_async_copy(a, b, load_sem.at[k]) for k, (a, b) in enumerate(zip(sources, local))]
-    for load in loads:
-        load.start()
     barrier = pltpu.get_barrier_semaphore()
     peers = [z_device(s) for s in DIRECT] + [y_device(s) for s in range(1, NY)]
     peers += [t_device(s) for s in range(1, NTP)]
     for peer in peers:
         pl.semaphore_signal(barrier, inc=1, device_id=peer, device_id_type=pl.DeviceIdType.MESH)
 
+    loads = [pltpu.make_async_copy(a, b, load_sem.at[k]) for k, (a, b) in enumerate(zip(sources, local))]
+    for load in loads:
+        load.start()
     for load in loads[:4]:
         load.wait()
     for h in both:
@@ -215,7 +215,7 @@
             ).start()
 
     loads[4].wait()
-    for step in ORDER[:7]:
+    for step in ORDER:
         chunk(step)
     loads[5].wait()
     held_weight[rows_of(z, y)] = weight[...].astype(BF)
@@ -228,7 +228,6 @@
     weights = Spread(held_weight, wsems, at, True)
     weights.begin()
     for step in ORDER[7:]:
-        chunk(step)
         chunk_out(0, step)
     for step in ORDER[7:]:
         chunk_out(1, step)

time: 63 us -> 63 us (level)
  no operation moved by 1% of the time
where the time goes in v5:
time: 63 us; the launch traced here: 62.9 us
  Pallas kernels  62.2 us (99%)
  between operations  0.64 us (1%)
    pallas_call x1, Pallas kernels, shards(): pl.pallas_call(kernel, out_shape=results, in_specs=[pl.BlockSpec(memory_s...  61.1 us

profile of v5, /device:TPU:2, one launch (start us, length us, event | category | flops | bytes accessed | tf_op | source)
XLA Modules:
  0.0 62.9 jit_solution(729425564425533238)
XLA Ops:
  0.6 61.1 %fused.1 = (f32[32,256]{1,0:T(8,128)S(1)}, f32[32,256]{1,0:T(8,128)S(1)}, bf16[2048,256]{1,0:T(8,128)(2,1)S(1)}, f32[32,256]{1,0:T(8,128)S(1)}, f32[2,128,128]{2,1,0:T(8,128)S(1)}) custom-call(bf16[128,256]{1,0:T(8,128)(2,1)} %refs_0_.1, bf16[128,256]{1,0:T(8,128)(2,1)} %refs_1_.1, f32[1,128]{1,0:T(1,128)} %bitcast.1, f32[2]{0:T(128)} %refs_3_.1, ...), custom_call_target="tpu_custom_call" | custom-call | tf_op jit(solution)/shard_map/fused/pallas_call | solution.py:471
  61.8 1.1 %store.1 = (f32[32,256]{1,0:T(8,128)}, f32[32,256]{1,0:T(8,128)}, bf16[2048,256]{1,0:T(8,128)(2,1)}, f32[32,256]{1,0:T(8,128)}, f32[2,128,128]{2,1,0:T(8,128)}) custom-call(f32[32,256]{1,0:T(8,128)S(1)} %get-tuple-element.10.refs_0_, f32[32,256]{1,0:T(8,128)S(1)} %get-tuple-element.11.refs_1_, bf16[2048,256]{1,0:T(8,128)(2,1)S(1)} %get-tuple-element.12.refs_2_, ...), custom_call_target="tpu_custom_call" | custom-call | tf_op jit(solution)/shard_map/store/pallas_call | solution.py:507
